TPU v7x, 32 devices: a whole 2x2x4 slice. The times are simulated.
32 devices in a mesh: ep: 8 (over z, y), tp: 4 (over x, core).
Axes of the slice: x: 2, y: 2, z: 4, core: 2. Of those that a mesh axis runs over, the one named last changes fastest.
Arguments:
- att_queries: bfloat16 [8192, 1024], P(('ep', 'tp')), may hold values from -8 to 8
- att_keys: bfloat16 [8192, 256], P(('ep', 'tp')), may hold values from -6 to 6
- att_values: bfloat16 [8192, 256], P(('ep', 'tp')), may hold values from -6 to 6
- sink_logits: float32 [16], replicated, may hold values from 3 to 6.5
- out_weight: bfloat16 [1024, 2048], replicated, may hold values from -0.1875 to 0.1875
- att_gain: float32 [2048], replicated, may hold values from 0.1 to 1.9
- moe_in: bfloat16 [4096, 2048], P(('ep', 'tp')), may hold values from -6 to 6
- pre_gain: float32 [2048], replicated, may hold values from 0.1 to 1.9
- expert_ids: int32 [4096, 2], P(('ep', 'tp')), may hold values from 0 to 15, all different within a row; in each aligned block of 128 rows (0 to 127, 128 to 255, ...) at most 32 rows name the same one
- routed_expert_weight: float32 [4096, 2], P(('ep', 'tp')), may hold values from 0.2 to 1.5
- w_gate: bfloat16 [16, 2048, 768], P('ep', None, 'tp'), may hold values from -0.125 to 0.125
- w_up: bfloat16 [16, 2048, 768], P('ep', None, 'tp'), may hold values from -0.125 to 0.125
- w_down: bfloat16 [16, 768, 2048], P('ep', 'tp'), may hold values from -0.21875 to 0.21875
- common_expert_gate_weight: bfloat16 [2048, 512], P(None, 'tp'), may hold values from -0.125 to 0.125
- common_expert_up_weight: bfloat16 [2048, 512], P(None, 'tp'), may hold values from -0.125 to 0.125
- common_expert_down_weight: bfloat16 [512, 2048], P('tp'), may hold values from -0.25 to 0.25
- moe_gain: float32 [2048], replicated, may hold values from 0.1 to 1.9
Outputs:
- mixer_out: bfloat16 [8192, 2048], P(('ep', 'tp'))
- experts_out: bfloat16 [4096, 2048], P(('ep', 'tp'))
Inputs may be any that keep to these rules, and one draw needn't show every extreme that they name: `expert_ids`: each row names 2 different experts; within the rows of one device no expert is named more than 32 times, and in every draw some expert is named exactly 32 times by the rows of some device.
All inputs are finite; a program needn't handle non-finite values.
Results may differ from a plain program's by a relative error of at most 0.012.
Values may be sent and summed in bfloat16 or wider, within the bound.
A program may use at most 128 MiB of HBM per device.

v0:
```python
import math
import jax
import jax.numpy as jnp
from jax import lax
from jax.sharding import PartitionSpec as P

HEADS = 16
KV_HEADS = 4
HEAD_DIM = 64
WINDOW = 128
EPS = 1e-06
NEGATIVE = -1e30


def from_behind(block, axis, distance):
    devices = range(lax.axis_size(axis))
    route = [(i - distance, i) for i in devices if i - distance in devices]
    return lax.ppermute(block, axis, route)


def rms_scale(inputs, gain_vec):
    mean_sq = jnp.mean(inputs * inputs, axis=-1, keepdims=True)
    return inputs * lax.rsqrt(mean_sq + EPS) * gain_vec


def slot_table(route_ids, slot_cap):
    flat_ids = route_ids.reshape(-1)
    assigned = flat_ids.shape[0]
    earlier = jnp.arange(assigned)[None, :] < jnp.arange(assigned)[:, None]
    position = jnp.sum((flat_ids[:, None] == flat_ids[None, :]) & earlier, axis=1)
    return (flat_ids * slot_cap + position).reshape(route_ids.shape)


def pack_rows(token_rows, slot_ids, slot_total):
    numbers = jnp.arange(slot_total, dtype=jnp.int32)
    chosen = jnp.any(slot_ids[None, :, :] == numbers[:, None, None], axis=2).astype(jnp.bfloat16)
    return jnp.dot(chosen, token_rows, preferred_element_type=jnp.float32).astype(jnp.bfloat16)


def body(
    att_queries,
    att_keys,
    att_values,
    sink_logits,
    out_weight,
    att_gain,
    moe_in,
    pre_gain,
    expert_ids,
    routed_expert_weight,
    w_gate,
    w_up,
    w_down,
    common_expert_gate_weight,
    common_expert_up_weight,
    common_expert_down_weight,
    moe_gain,
):
    tok_rows = att_queries.shape[0]
    group_size = HEADS // KV_HEADS
    blocks = tok_rows // WINDOW
    kv_rows = jnp.stack([att_keys, att_values])
    rim_rows = from_behind(kv_rows[:, tok_rows - WINDOW :], ("ep", "tp"), 1)
    kv_all = jnp.concatenate([rim_rows, kv_rows], axis=1).reshape(
        2, blocks + 1, WINDOW, KV_HEADS, HEAD_DIM
    )
    kv_band = jnp.concatenate([kv_all[:, :-1], kv_all[:, 1:]], axis=2)
    query_blocks = att_queries.reshape(blocks, WINDOW, KV_HEADS, group_size, HEAD_DIM)
    scores = jnp.einsum(
        "nqgjd,nkgd->ngjqk", query_blocks, kv_band[0], preferred_element_type=jnp.float32
    ) * (1.0 / math.sqrt(HEAD_DIM))
    distance = jnp.arange(WINDOW)[:, None] + WINDOW - jnp.arange(2 * WINDOW)[None, :]
    inside = (distance >= 0) & (distance < WINDOW)
    first_pos = lax.axis_index(("ep", "tp")) * tok_rows
    key_pos = (
        first_pos + jnp.arange(blocks)[:, None] * WINDOW - WINDOW + jnp.arange(2 * WINDOW)[None, :]
    )
    is_valid = inside[None] & (key_pos >= 0)[:, None, :]
    scores = jnp.where(is_valid[:, None, None], scores, NEGATIVE)
    sink_grid = sink_logits.reshape(KV_HEADS, group_size)[None, :, :, None, None]
    row_top = jnp.maximum(jnp.max(scores, axis=-1, keepdims=True), sink_grid)
    exp_scores = jnp.exp(scores - row_top)
    denominator = jnp.sum(exp_scores, axis=-1, keepdims=True) + jnp.exp(sink_grid - row_top)
    probs = (exp_scores / denominator).astype(jnp.bfloat16)
    head_mix = jnp.einsum(
        "ngjqk,nkgd->nqgjd", probs, kv_band[1], preferred_element_type=jnp.float32
    )
    head_mix = head_mix.astype(jnp.bfloat16).reshape(tok_rows, HEADS * HEAD_DIM)
    projected = jnp.dot(head_mix, out_weight, preferred_element_type=jnp.float32)
    mixer_out = rms_scale(projected, att_gain).astype(jnp.bfloat16)
    tokens = moe_in.shape[0]
    top_count = expert_ids.shape[1]
    local_experts = w_gate.shape[0]
    ep_size = lax.axis_size("ep")
    tp_size = lax.axis_size("tp")
    experts = local_experts * ep_size
    slot_cap = 2 * tokens * top_count // experts
    slot_total = experts * slot_cap
    normed = rms_scale(moe_in.astype(jnp.float32), pre_gain).astype(jnp.bfloat16)
    own_slots = slot_table(expert_ids, slot_cap)
    packed = pack_rows(normed, own_slots, slot_total)[None]
    arrived = lax.all_to_all(packed, "ep", split_axis=1, concat_axis=1, tiled=True)
    arrived_all, tokens_all = (
        lax.all_gather(arrived[0], "tp", axis=0, tiled=True),
        lax.all_gather(normed, "tp", axis=0, tiled=True),
    )
    arrived = arrived_all.reshape(tp_size, slot_total, normed.shape[1])
    token_block = tokens_all.reshape(tp_size, tokens, normed.shape[1])
    routed = arrived
    routed = routed.reshape(
        1 * lax.axis_size("tp"), ep_size, local_experts, slot_cap, normed.shape[1]
    )
    gate_act = jnp.einsum("tsjcd,jdf->tsjcf", routed, w_gate, preferred_element_type=jnp.float32)
    up_act = jnp.einsum("tsjcd,jdf->tsjcf", routed, w_up, preferred_element_type=jnp.float32)
    hidden = (jax.nn.silu(gate_act) * up_act).astype(jnp.bfloat16)
    routed_part = jnp.einsum("tsjcf,jfd->tsjcd", hidden, w_down, preferred_element_type=jnp.float32)
    routed_part = routed_part.reshape(1 * lax.axis_size("tp"), slot_total, normed.shape[1])
    common_gate_activation = jnp.einsum(
        "spz,zv->spv", token_block, common_expert_gate_weight, preferred_element_type=jnp.float32
    )
    shared_up_act = jnp.einsum(
        "spz,zv->spv", token_block, common_expert_up_weight, preferred_element_type=jnp.float32
    )
    common_expert_hidden = (jax.nn.silu(common_gate_activation) * shared_up_act).astype(
        jnp.bfloat16
    )
    shared_part = jnp.einsum(
        "nsq,ql->nsl",
        common_expert_hidden,
        common_expert_down_weight,
        preferred_element_type=jnp.float32,
    )
    summed = lax.psum_scatter(
        jnp.concatenate([routed_part, shared_part], axis=1).astype(jnp.bfloat16),
        "tp",
        scatter_dimension=0,
        tiled=True,
    ).astype(jnp.float32)
    routed_out = summed[0, :slot_total].astype(jnp.bfloat16)
    shared_sum = summed[0, slot_total:]
    returned = lax.all_to_all(routed_out, "ep", split_axis=0, concat_axis=0, tiled=True)
    picked = returned[own_slots.reshape(-1)].reshape(tokens, top_count, normed.shape[1])
    combined = (
        jnp.sum(routed_expert_weight[:, :, None] * picked.astype(jnp.float32), axis=1) + shared_sum
    )
    experts_out = rms_scale(combined, moe_gain).astype(jnp.bfloat16)
    return (mixer_out, experts_out)


def solution(mesh):
    in_specs = (
        P(("ep", "tp"), None),
        P(("ep", "tp"), None),
        P(("ep", "tp"), None),
        P(),
        P(),
        P(),
        P(("ep", "tp"), None),
        P(),
        P(("ep", "tp"), None),
        P(("ep", "tp"), None),
        P("ep", None, "tp"),
        P("ep", None, "tp"),
        P("ep", "tp", None),
        P(None, "tp"),
        P(None, "tp"),
        P("tp", None),
        P(),
    )
    out_specs = (P(("ep", "tp"), None), P(("ep", "tp"), None))
    return jax.shard_map(body, mesh=mesh, in_specs=in_specs, out_specs=out_specs, check_vma=False)
```

profile of v0, /device:TPU:0, one launch (start us, length us, event | category | flops | bytes accessed | tf_op | source)
XLA Modules:
  0.0 362.7 jit_solution(12713361354934625359)
XLA Ops:
  11.9 5.2 %copy.111 = bf16[1,512,2048]{2,0,1:T(2,128)(2,1)} copy(bf16[1,512,2048]{2,1,0:T(8,128)(2,1)S(1)} %fusion.6) | data formatting | bytes 4194304 | tf_op jit(solution)/shard_map/broadcast_in_dim | solution.py:101
  17.6 14.5 %reduce = bf16[512,2048]{1,0:T(8,128)(2,1)} reduce(bf16[512,1,2048]{2,1,0:T(2,128)(2,1)} %bitcast.116, bf16[]{:T(256)} %broadcast.169), dimensions={1}, to_apply=%bitcast.113.reduce_sub_computation | reduce | bytes 4194306
  32.1 6.3 %reshape.191 = bf16[8,2,65536]{2,1,0:T(2,128)(2,1)} reshape(bf16[512,2048]{1,0:T(8,128)(2,1)} %reduce) | data formatting | bytes 4194304
  38.4 7.3 %all-to-all-start = ((bf16[8,2,65536]{2,1,0:T(2,128)(2,1)}), bf16[8,2,65536]{2,1,0:T(2,128)(2,1)}, u32[]{:S(2)}, u32[]{:S(2)}) async-start(bf16[8,2,65536]{2,1,0:T(2,128)(2,1)} %reshape.191), calls=%async_computation | async-start | bytes 4194304 | tf_op jit(solution)/shard_map/all_to_all | solution.py:102
  46.5 47.6 %all-to-all-done = bf16[8,2,65536]{2,1,0:T(2,128)(2,1)} async-done(((bf16[8,2,65536]{2,1,0:T(2,128)(2,1)}), bf16[8,2,65536]{2,1,0:T(2,128)(2,1)}, u32[]{:S(2)}, u32[]{:S(2)}) %all-to-all-start) | async-done | bytes 2097184 | tf_op jit(solution)/shard_map/all_to_all | solution.py:102
  94.1 6.8 %reshape.192 = bf16[512,1,2048]{2,1,0:T(2,128)(2,1)} reshape(bf16[8,2,65536]{2,1,0:T(2,128)(2,1)} %all-to-all-done) | data formatting | bytes 4194304
  100.8 4.8 %copy.75 = bf16[1,512,2048]{2,1,0:T(8,128)(2,1)} copy(bf16[1,512,2048]{2,0,1:T(2,128)(2,1)} %bitcast.117) | data formatting | bytes 4194304 | tf_op jit(solution)/shard_map/all_to_all | solution.py:102
  106.6 2.3 fusion.35
  108.9 5.2 %convolution_convert_fusion = bf16[4,128,2048]{2,1,0:T(8,128)(2,1)} fusion(bf16[4,128,2048]{2,1,0:T(8,128)(2,1)} %bitcast.120, bf16[128,2048]{1,0:T(8,128)(2,1)S(1)} %copy-done.8, bf16[2048,128]{1,0:T(8,128)(2,1)S(1)} %copy-done.9, f32[4,128,128]{2,1,0:T(8,128)S(1)} %fusion.35), kind=kOutput, calls=%fused_computation.12 | convolution fusion | flops 538312704 | bytes 5505024 | tf_op jit(solution)/shard_map/nsq,ql->nsl/dot_general | solution.py:127
  114.2 48.9 %all-gather.6.cloned.1.call-done = bf16[1,2048,2048]{2,1,0:T(8,128)(2,1)} async-done(((bf16[1,512,2048]{2,1,0:T(8,128)(2,1)}), bf16[1,2048,2048]{2,1,0:T(8,128)(2,1)}) %all-gather.6.cloned.1.call-update) | async-done | bytes 8388624 | tf_op jit(solution)/shard_map/all_gather | solution.py:104
  163.1 7.6 %fusion.2 = f32[2,4,8,32,192]{4,3,2,1,0:T(8,128)} fusion(bf16[4,8,2,32,2048]{4,3,2,1,0:T(8,128)(2,1)} %bitcast.128, bf16[2,2048,192]{1,2,0:T(8,128)(2,1)} %param.27), kind=kOutput, calls=%fused_computation.5 | convolution fusion | flops 1610612736 | bytes 11534336 | tf_op jit(solution)/shard_map/tsjcd,jdf->tsjcf/dot_general | solution.py:113
  170.7 13.2 %convert_bitcast_fusion = bf16[4,8,2,32,2048]{4,3,1,0,2:T(8,128)(2,1)} fusion(f32[2,4,8,32,192]{4,3,2,1,0:T(8,128)} %fusion.2, bf16[4,8,2,32,2048]{4,3,2,1,0:T(8,128)(2,1)} %bitcast.129, bf16[2,192,2048]{2,1,0:T(8,128)(2,1)S(1)} %copy-done, bf16[2,2048,192]{1,2,0:T(8,128)(2,1)S(1)} %copy-done.15), kind=kOutput, calls=%fused_computation.2 | convolution fusion | flops 3227779072 | bytes 21495808 | tf_op jit(solution)/shard_map/tsjcf,jfd->tsjcd/dot_general | solution.py:116
  183.8 8.4 %copy.78 = bf16[4,8,2,32,2048]{4,3,2,1,0:T(8,128)(2,1)} copy(bf16[4,8,2,32,2048]{4,3,1,0,2:T(8,128)(2,1)} %convert_bitcast_fusion) | data formatting | bytes 16777216 | tf_op jit(solution)/shard_map/tsjcf,jfd->tsjcd/transpose | solution.py:116
  192.3 10.5 %pad_maximum_fusion = bf16[4,640,2048]{2,1,0:T(8,128)(2,1)} fusion(bf16[4,128,2048]{2,1,0:T(8,128)(2,1)S(1)} %copy-done.2, bf16[4,512,2048]{2,1,0:T(8,128)(2,1)} %bitcast.115), kind=kLoop, calls=%fused_computation.1 | loop fusion | flops 20971520 | bytes 20971520 | tf_op jit(solution)/shard_map/concatenate | solution.py:134
  203.7 2.8 collective-permute-start
  206.9 80.4 %reduce-scatter.2.cloned.1.call-done = bf16[1,640,2048]{2,1,0:T(8,128)(2,1)} async-done(((bf16[4,640,2048]{2,1,0:T(8,128)(2,1)}), bf16[1,640,2048]{2,1,0:T(8,128)(2,1)}) %reduce-scatter.2.cloned.1.call-update) | async-done | bytes 2621456 | tf_op jit(solution)/shard_map/reduce_scatter | solution.py:133
  287.3 3.2 slice.36
  290.5 5.6 %all-to-all-start.1 = ((bf16[8,64,2048]{2,1,0:T(8,128)(2,1)}), bf16[8,64,2048]{2,1,0:T(8,128)(2,1)S(1)}, u32[]{:S(2)}, u32[]{:S(2)}) async-start(bf16[8,64,2048]{2,1,0:T(8,128)(2,1)} %bitcast.118), calls=%async_computation.2 | async-start | bytes 4194304 | tf_op jit(solution)/shard_map/all_to_all | solution.py:141
  296.1 1.6 reshape.189
  301.9 2.1 fusion.5
  310.0 34.2 %all-to-all-done.1 = bf16[8,64,2048]{2,1,0:T(8,128)(2,1)S(1)} async-done(((bf16[8,64,2048]{2,1,0:T(8,128)(2,1)}), bf16[8,64,2048]{2,1,0:T(8,128)(2,1)S(1)}, u32[]{:S(2)}, u32[]{:S(2)}) %all-to-all-start.1) | async-done | bytes 2097184 | tf_op jit(solution)/shard_map/all_to_all | solution.py:141
  345.6 2.3 reshape.169
  347.9 4.9 %multiply_reduce_fusion = f32[128,2048]{1,0:T(8,128)S(1)} fusion(f32[128,2,2048]{2,1,0:T(2,128)} %reshape.169, f32[128,2]{1,0:T(8,128)S(1)} %copy.70), kind=kLoop, calls=%fused_computation.22 | loop fusion | flops 786432 | bytes 3146752 | tf_op jit(solution)/shard_map/reduce_sum | solution.py:144
  354.2 2.0 multiply_convert_fusion.1
  (79 shorter events, 21.0 us)
Async XLA Ops:
  7.2 163.5 %copy-start = (bf16[2,192,2048]{2,1,0:T(8,128)(2,1)S(1)}, bf16[2,192,2048]{2,1,0:T(8,128)(2,1)}, u32[]{:S(2)}) copy-start(bf16[2,192,2048]{2,1,0:T(8,128)(2,1)} %param.29) | copy-start | bytes 4718596
  11.2 5.9 %copy-start.3 = (bf16[128,2048]{1,0:T(8,128)(2,1)}, bf16[128,2048]{1,0:T(8,128)(2,1)S(1)}, u32[]{:S(2)}) copy-start(bf16[128,2048]{1,0:T(8,128)(2,1)S(1)} %fusion.25) | copy-start | bytes 1572868
  38.4 55.7 %all-to-all-start = ((bf16[8,2,65536]{2,1,0:T(2,128)(2,1)}), bf16[8,2,65536]{2,1,0:T(2,128)(2,1)}, u32[]{:S(2)}, u32[]{:S(2)}) async-start(bf16[8,2,65536]{2,1,0:T(2,128)(2,1)} %reshape.191), calls=%async_computation | async-start | bytes 4194304 | tf_op jit(solution)/shard_map/all_to_all | solution.py:102
  45.7 60.1 %all-gather.4.cloned.1.call-start = ((), (), s32[]{:S(2)}) async-start(), calls=%async_computation.3 | async-start | bytes 2621440 | tf_op jit(solution)/shard_map/all_gather | solution.py:105
  46.4 116.6 %all-gather.6.cloned.1.call-start = ((), (), s32[]{:S(2)}) async-start(), calls=%async_computation.5 | async-start | bytes 10485760 | tf_op jit(solution)/shard_map/all_gather | solution.py:104
  105.6 1.0 copy-start.7
  105.6 3.3 copy-start.8
  105.6 3.3 copy-start.9
  105.6 181.7 %reduce-scatter.2.cloned.1.call-start = ((), (), s32[]{:S(2)}) async-start(), calls=%async_computation.4 | async-start | bytes 13107200 | tf_op jit(solution)/shard_map/reduce_scatter | solution.py:133
  163.1 7.6 %copy-start.15 = (bf16[2,2048,192]{1,2,0:T(8,128)(2,1)S(1)}, bf16[2,2048,192]{1,2,0:T(8,128)(2,1)}, u32[]{:S(2)}) copy-start(bf16[2,2048,192]{1,2,0:T(8,128)(2,1)} %param.28) | copy-start | bytes 4718596
  183.8 8.4 %copy-start.2 = (bf16[4,128,2048]{2,1,0:T(8,128)(2,1)S(1)}, bf16[4,128,2048]{2,1,0:T(8,128)(2,1)}, u32[]{:S(2)}) copy-start(bf16[4,128,2048]{2,1,0:T(8,128)(2,1)} %convolution_convert_fusion) | copy-start | bytes 6291460
  202.7 0.9 copy-start.5
  202.7 1.0 copy-start.6
  203.7 94.3 %collective-permute-start = (bf16[2,128,256]{2,1,0:T(8,128)(2,1)S(1)}, bf16[2,128,256]{2,1,0:T(8,128)(2,1)}, u32[]{:S(2)}, u32[]{:S(2)}) collective-permute-start(bf16[2,128,256]{2,1,0:T(8,128)(2,1)S(1)} %pad_maximum_fusion.2), channel_id=1, source_target_pairs={{0,1},{1,2},{2,3},{3,4},{4,5},{5,6},{6,7},{7,8},{8,9},{9,10},{10,1... | collective-permute-start | bytes 393224 | tf_op jit(solution)/shard_map/ppermute | solution.py:18
  290.5 5.7 %copy-start.4 = (bf16[256,1024]{1,0:T(8,128)(2,1)S(1)}, bf16[256,1024]{1,0:T(8,128)(2,1)}, u32[]{:S(2)}) copy-start(bf16[256,1024]{1,0:T(8,128)(2,1)} %param.17) | copy-start | bytes 1572868
  290.5 7.3 %copy-start.13 = (f32[16]{0:T(128)S(1)}, f32[16]{0:T(128)}, u32[]{:S(2)}) copy-start(f32[16]{0:T(128)} %param.20) | copy-start | bytes 196
  290.5 7.4 %copy-start.12 = (f32[128,2]{0,1:T(2,128)S(1)}, f32[128,2]{0,1:T(2,128)}, u32[]{:S(2)}) copy-start(f32[128,2]{0,1:T(2,128)} %param.26) | copy-start | bytes 3076
  290.5 53.7 %all-to-all-start.1 = ((bf16[8,64,2048]{2,1,0:T(8,128)(2,1)}), bf16[8,64,2048]{2,1,0:T(8,128)(2,1)S(1)}, u32[]{:S(2)}, u32[]{:S(2)}) async-start(bf16[8,64,2048]{2,1,0:T(8,128)(2,1)} %bitcast.118), calls=%async_computation.2 | async-start | bytes 4194304 | tf_op jit(solution)/shard_map/all_to_all | solution.py:141
  305.2 2.2 copy-start.14
  307.4 1.4 copy-start.10
  347.9 6.2 %copy-start.11 = (f32[2048]{0:T(1024)S(1)}, f32[2048]{0:T(1024)}, u32[]{:S(2)}) copy-start(f32[2048]{0:T(1024)} %param.33) | copy-start | bytes 24580
  347.9 8.3 %copy-start.1 = (bf16[2,192,2048]{2,1,0:T(8,128)(2,1)S(1)}, bf16[2,192,2048]{2,1,0:T(8,128)(2,1)}, u32[]{:S(2)}) copy-start(bf16[2,192,2048]{2,1,0:T(8,128)(2,1)} %param.29) | copy-start | bytes 4718596
Sparse Core Ops, SparseCore 0:
  48.7 23.9 all-gather.3
  105.7 57.2 all-gather.5
  202.9 84.3 reduce-scatter.1
where the time goes:
time: 364 us; the launch traced here: 363 us
  waiting for transfers between devices  212 us (58%)
  local copies, waits for them, and re-layouts  47.7 us (13%)
  other arithmetic  39.5 us (11%)
  matrix products  33.7 us (9%)
  starting transfers between devices  16.1 us (4%)
  between operations  14 us (4%)
    reduce_scatter x1, waiting for transfers between devices, body(): lax.psum_scatter(jnp.concatenate([routed_part, shared_part], axis=1).asty...  80.4 us
    all_gather x1, waiting for transfers between devices, body(): lax.all_gather(arrived[0], 'tp', axis=0, tiled=True)  48.9 us
    all_to_all x1, waiting for transfers between devices, body(): lax.all_to_all(packed, 'ep', split_axis=1, concat_axis=1, tiled=True)  47.6 us
    all_to_all x1, waiting for transfers between devices, body(): lax.all_to_all(routed_out, 'ep', split_axis=0, concat_axis=0, tiled=True)  34.2 us
    unnamed x39, local copies, waits for them, and re-layouts  18.3 us
    unnamed x1, other arithmetic  14.5 us
    dot_general x1, matrix products, body(): jnp.einsum('tsjcf,jfd->tsjcd', hidden, w_down, preferred_element_type=jnp...  13.2 us
    concatenate x1, other arithmetic, body(): jnp.concatenate([routed_part, shared_part], axis=1).astype(jnp.bfloat16)  10.5 us
  transfers between devices with their start and end apart: 6, of which 4 were waited for; matrix products, arithmetic and copies ran while one was open for 10% of the time, Pallas kernels for 0%

commit v1 on v0

--- a/solution.py
+++ b/solution.py
@@ -99,7 +99,10 @@
     normed = rms_scale(moe_in.astype(jnp.float32), pre_gain).astype(jnp.bfloat16)
     own_slots = slot_table(expert_ids, slot_cap)
     packed = pack_rows(normed, own_slots, slot_total)[None]
-    arrived = lax.all_to_all(packed, "ep", split_axis=1, concat_axis=1, tiled=True)
+    size = lax.axis_size("ep")
+    pieces = jnp.stack(jnp.split(packed, size, axis=1), axis=0)
+    pieces = lax.all_to_all(pieces, "ep", split_axis=0, concat_axis=0)
+    arrived = jnp.concatenate(pieces, axis=1)
     arrived_all, tokens_all = (
         lax.all_gather(arrived[0], "tp", axis=0, tiled=True),
         lax.all_gather(normed, "tp", axis=0, tiled=True),

time: 364 us -> 331 us (0.909)
  local copies, waits for them, and re-layouts: 47.7 us -> 29.2 us
  other arithmetic: 39.5 us -> 25 us
    unnamed x1 -> x0, other arithmetic: 14.5 us -> none
    unnamed x39 -> x43, local copies, waits for them, and re-layouts: 18.3 us -> 8.98 us
    broadcast_in_dim x1 -> x0, local copies, waits for them, and re-layouts: 5.17 us -> none  [body(): packed = pack_rows(normed, own_slots, slot_total)[None]]
    all_to_all x1 -> x0, local copies, waits for them, and re-layouts: 4.77 us -> none  [body(): lax.all_to_all(packed, 'ep', split_axis=1, concat_axis=1, tiled=True)]
  transfers between devices with their start and end apart: 6 -> 6, of which waited for: 4 -> 4; matrix products, arithmetic and copies ran while one was open for 10% -> 7% of each run, Pallas kernels for 0% -> 0%
where the time goes in v1:
time: 331 us
  waiting for transfers between devices  213 us (64%)
  matrix products  33.8 us (10%)
  local copies, waits for them, and re-layouts  29.2 us (9%)
  other arithmetic  25 us (8%)
  starting transfers between devices  15.9 us (5%)
  between operations  14 us (4%)
    reduce_scatter x1, waiting for transfers between devices, body(): lax.psum_scatter(jnp.concatenate([routed_part, shared_part], axis=1).asty...  80.4 us
    all_gather x1, waiting for transfers between devices, body(): lax.all_gather(arrived[0], 'tp', axis=0, tiled=True)  49.7 us
    all_to_all x1, waiting for transfers between devices, body(): pieces = lax.all_to_all(pieces, 'ep', split_axis=0, concat_axis=0)  47.6 us
    all_to_all x1, waiting for transfers between devices, body(): lax.all_to_all(routed_out, 'ep', split_axis=0, concat_axis=0, tiled=True)  34.2 us
    dot_general x1, matrix products, body(): jnp.einsum('tsjcf,jfd->tsjcd', hidden, w_down, preferred_element_type=jnp...  13.2 us
    concatenate x1, other arithmetic, body(): jnp.concatenate([routed_part, shared_part], axis=1).astype(jnp.bfloat16)  10.4 us
    unnamed x43, local copies, waits for them, and re-layouts  8.98 us
    transpose x1, local copies, waits for them, and re-layouts, body(): jnp.einsum('tsjcf,jfd->tsjcd', hidden, w_down, preferred_element_type=jnp...  8.43 us
  transfers between devices with their start and end apart: 6, of which 4 were waited for; matrix products, arithmetic and copies ran while one was open for 7% of the time, Pallas kernels for 0%

profile of v1, /device:TPU:0, one launch (start us, length us, event | category | flops | bytes accessed | tf_op | source)
XLA Modules:
  0.0 330.5 jit_solution(4239750972461434371)
XLA Ops:
  10.0 1.2 fusion.25
  17.6 7.3 %all-to-all-start = ((bf16[8,1,64,2048]{3,2,1,0:T(8,128)(2,1)}), bf16[8,1,64,2048]{3,2,1,0:T(8,128)(2,1)}, u32[]{:S(2)}, u32[]{:S(2)}) async-start(bf16[8,1,64,2048]{3,2,1,0:T(8,128)(2,1)} %fusion.41), calls=%async_computation | async-start | bytes 4194304 | tf_op jit(solution)/shard_map/all_to_all | solution.py:104
  25.7 47.6 %all-to-all-done = bf16[8,1,64,2048]{3,2,1,0:T(8,128)(2,1)} async-done(((bf16[8,1,64,2048]{3,2,1,0:T(8,128)(2,1)}), bf16[8,1,64,2048]{3,2,1,0:T(8,128)(2,1)}, u32[]{:S(2)}, u32[]{:S(2)}) %all-to-all-start) | async-done | bytes 2097184 | tf_op jit(solution)/shard_map/all_to_all | solution.py:104
  73.4 2.4 fusion.35
  75.8 5.3 %convolution_convert_fusion = bf16[4,128,2048]{2,1,0:T(8,128)(2,1)} fusion(bf16[4,128,2048]{2,1,0:T(8,128)(2,1)} %bitcast.147, bf16[128,2048]{1,0:T(8,128)(2,1)S(1)} %copy-done.8, bf16[2048,128]{1,0:T(8,128)(2,1)S(1)} %copy-done.9, f32[4,128,128]{2,1,0:T(8,128)S(1)} %fusion.35), kind=kOutput, calls=%fused_computation.12 | convolution fusion | flops 538312704 | bytes 5505024 | tf_op jit(solution)/shard_map/nsq,ql->nsl/dot_general | solution.py:130
  81.1 49.7 %all-gather.3.cloned.1.call-done = bf16[2048,2048]{1,0:T(8,128)(2,1)} async-done(((bf16[512,2048]{1,0:T(8,128)(2,1)}), bf16[2048,2048]{1,0:T(8,128)(2,1)}) %all-gather.3.cloned.1.call-update) | async-done | bytes 8388624 | tf_op jit(solution)/shard_map/all_gather | solution.py:107
  130.8 7.6 %fusion.2 = f32[2,4,8,32,192]{4,3,2,1,0:T(8,128)} fusion(bf16[4,8,2,32,2048]{4,3,2,1,0:T(8,128)(2,1)} %bitcast.155, bf16[2,2048,192]{1,2,0:T(8,128)(2,1)} %param.27), kind=kOutput, calls=%fused_computation.5 | convolution fusion | flops 1610612736 | bytes 11534336 | tf_op jit(solution)/shard_map/tsjcd,jdf->tsjcf/dot_general | solution.py:116
  138.4 13.2 %convert_bitcast_fusion = bf16[4,8,2,32,2048]{4,3,1,0,2:T(8,128)(2,1)} fusion(f32[2,4,8,32,192]{4,3,2,1,0:T(8,128)} %fusion.2, bf16[4,8,2,32,2048]{4,3,2,1,0:T(8,128)(2,1)} %bitcast.156, bf16[2,192,2048]{2,1,0:T(8,128)(2,1)S(1)} %copy-done, bf16[2,2048,192]{1,2,0:T(8,128)(2,1)S(1)} %copy-done.15), kind=kOutput, calls=%fused_computation.2 | convolution fusion | flops 3227779072 | bytes 21495808 | tf_op jit(solution)/shard_map/tsjcf,jfd->tsjcd/dot_general | solution.py:119
  151.6 8.4 %copy.48 = bf16[4,8,2,32,2048]{4,3,2,1,0:T(8,128)(2,1)} copy(bf16[4,8,2,32,2048]{4,3,1,0,2:T(8,128)(2,1)} %convert_bitcast_fusion) | data formatting | bytes 16777216 | tf_op jit(solution)/shard_map/tsjcf,jfd->tsjcd/transpose | solution.py:119
  160.0 10.4 %pad_maximum_fusion = bf16[4,640,2048]{2,1,0:T(8,128)(2,1)} fusion(bf16[4,128,2048]{2,1,0:T(8,128)(2,1)S(1)} %copy-done.2, bf16[4,512,2048]{2,1,0:T(8,128)(2,1)} %bitcast.144), kind=kLoop, calls=%fused_computation.1 | loop fusion | flops 20971520 | bytes 20971520 | tf_op jit(solution)/shard_map/concatenate | solution.py:137
  171.4 2.8 collective-permute-start
  174.7 80.4 %reduce-scatter.2.cloned.1.call-done = bf16[1,640,2048]{2,1,0:T(8,128)(2,1)} async-done(((bf16[4,640,2048]{2,1,0:T(8,128)(2,1)}), bf16[1,640,2048]{2,1,0:T(8,128)(2,1)}) %reduce-scatter.2.cloned.1.call-update) | async-done | bytes 2621456 | tf_op jit(solution)/shard_map/reduce_scatter | solution.py:136
  255.0 3.2 slice.36
  258.2 5.7 %all-to-all-start.1 = ((bf16[8,64,2048]{2,1,0:T(8,128)(2,1)}), bf16[8,64,2048]{2,1,0:T(8,128)(2,1)S(1)}, u32[]{:S(2)}, u32[]{:S(2)}) async-start(bf16[8,64,2048]{2,1,0:T(8,128)(2,1)} %bitcast.145), calls=%async_computation.2 | async-start | bytes 4194304 | tf_op jit(solution)/shard_map/all_to_all | solution.py:144
  264.0 1.6 reshape.187
  268.2 1.3 copy.59
  269.7 2.1 fusion.5
  275.2 1.4 multiply_reduce_fusion.1
  277.8 34.2 %all-to-all-done.1 = bf16[8,64,2048]{2,1,0:T(8,128)(2,1)S(1)} async-done(((bf16[8,64,2048]{2,1,0:T(8,128)(2,1)}), bf16[8,64,2048]{2,1,0:T(8,128)(2,1)S(1)}, u32[]{:S(2)}, u32[]{:S(2)}) %all-to-all-start.1) | async-done | bytes 2097184 | tf_op jit(solution)/shard_map/all_to_all | solution.py:144
  312.0 1.4 gather_fusion
  313.3 2.4 reshape.169
  315.7 4.9 %multiply_reduce_fusion = f32[128,2048]{1,0:T(8,128)S(1)} fusion(f32[128,2,2048]{2,1,0:T(2,128)} %reshape.169, f32[128,2]{1,0:T(8,128)S(1)} %copy.42), kind=kLoop, calls=%fused_computation.22 | loop fusion | flops 786432 | bytes 3146752 | tf_op jit(solution)/shard_map/reduce_sum | solution.py:147
  320.6 1.3 multiply_reduce_fusion.2
  321.9 2.0 multiply_convert_fusion.1
  (81 shorter events, 18.8 us)
Async XLA Ops:
  7.2 131.2 %copy-start = (bf16[2,192,2048]{2,1,0:T(8,128)(2,1)S(1)}, bf16[2,192,2048]{2,1,0:T(8,128)(2,1)}, u32[]{:S(2)}) copy-start(bf16[2,192,2048]{2,1,0:T(8,128)(2,1)} %param.29) | copy-start | bytes 4718596
  11.2 2.9 copy-start.3
  17.6 55.7 %all-to-all-start = ((bf16[8,1,64,2048]{3,2,1,0:T(8,128)(2,1)}), bf16[8,1,64,2048]{3,2,1,0:T(8,128)(2,1)}, u32[]{:S(2)}, u32[]{:S(2)}) async-start(bf16[8,1,64,2048]{3,2,1,0:T(8,128)(2,1)} %fusion.41), calls=%async_computation | async-start | bytes 4194304 | tf_op jit(solution)/shard_map/all_to_all | solution.py:104
  25.0 48.4 %copy-start.7 = (bf16[2048,128]{1,0:T(8,128)(2,1)S(1)}, bf16[2048,128]{1,0:T(8,128)(2,1)}, u32[]{:S(2)}) copy-start(bf16[2048,128]{1,0:T(8,128)(2,1)} %param.30) | copy-start | bytes 1572868
  25.0 48.4 %all-gather.5.cloned.1.call-start = ((), (), s32[]{:S(2)}) async-start(), calls=%async_computation.4 | async-start | bytes 2621440 | tf_op jit(solution)/shard_map/all_gather | solution.py:108
  25.7 105.1 %all-gather.3.cloned.1.call-start = ((), (), s32[]{:S(2)}) async-start(), calls=%async_computation.3 | async-start | bytes 10485760 | tf_op jit(solution)/shard_map/all_gather | solution.py:107
  73.3 2.5 copy-start.8
  73.3 2.5 copy-start.9
  73.3 181.7 %reduce-scatter.2.cloned.1.call-start = ((), (), s32[]{:S(2)}) async-start(), calls=%async_computation.5 | async-start | bytes 13107200 | tf_op jit(solution)/shard_map/reduce_scatter | solution.py:136
  130.8 7.6 %copy-start.15 = (bf16[2,2048,192]{1,2,0:T(8,128)(2,1)S(1)}, bf16[2,2048,192]{1,2,0:T(8,128)(2,1)}, u32[]{:S(2)}) copy-start(bf16[2,2048,192]{1,2,0:T(8,128)(2,1)} %param.28) | copy-start | bytes 4718596
  151.6 8.4 %copy-start.2 = (bf16[4,128,2048]{2,1,0:T(8,128)(2,1)S(1)}, bf16[4,128,2048]{2,1,0:T(8,128)(2,1)}, u32[]{:S(2)}) copy-start(bf16[4,128,2048]{2,1,0:T(8,128)(2,1)} %convolution_convert_fusion) | copy-start | bytes 6291460
  170.5 0.9 copy-start.5
  170.5 1.0 copy-start.6
  171.4 94.3 %collective-permute-start = (bf16[2,128,256]{2,1,0:T(8,128)(2,1)S(1)}, bf16[2,128,256]{2,1,0:T(8,128)(2,1)}, u32[]{:S(2)}, u32[]{:S(2)}) collective-permute-start(bf16[2,128,256]{2,1,0:T(8,128)(2,1)S(1)} %pad_maximum_fusion.2), channel_id=1, source_target_pairs={{0,1},{1,2},{2,3},{3,4},{4,5},{5,6},{6,7},{7,8},{8,9},{9,10},{10,1... | collective-permute-start | bytes 393224 | tf_op jit(solution)/shard_map/ppermute | solution.py:18
  258.2 5.7 %copy-start.12 = (f32[128,2]{0,1:T(2,128)S(1)}, f32[128,2]{0,1:T(2,128)}, u32[]{:S(2)}) copy-start(f32[128,2]{0,1:T(2,128)} %param.26) | copy-start | bytes 3076
  258.2 5.8 %copy-start.4 = (bf16[256,1024]{1,0:T(8,128)(2,1)S(1)}, bf16[256,1024]{1,0:T(8,128)(2,1)}, u32[]{:S(2)}) copy-start(bf16[256,1024]{1,0:T(8,128)(2,1)} %param.17) | copy-start | bytes 1572868
  258.2 7.4 %copy-start.13 = (f32[16]{0:T(128)S(1)}, f32[16]{0:T(128)}, u32[]{:S(2)}) copy-start(f32[16]{0:T(128)} %param.20) | copy-start | bytes 196
  258.2 53.7 %all-to-all-start.1 = ((bf16[8,64,2048]{2,1,0:T(8,128)(2,1)}), bf16[8,64,2048]{2,1,0:T(8,128)(2,1)S(1)}, u32[]{:S(2)}, u32[]{:S(2)}) async-start(bf16[8,64,2048]{2,1,0:T(8,128)(2,1)} %bitcast.145), calls=%async_computation.2 | async-start | bytes 4194304 | tf_op jit(solution)/shard_map/all_to_all | solution.py:144
  273.0 2.2 copy-start.14
  275.2 1.4 copy-start.10
  315.7 6.2 %copy-start.11 = (f32[2048]{0:T(1024)S(1)}, f32[2048]{0:T(1024)}, u32[]{:S(2)}) copy-start(f32[2048]{0:T(1024)} %param.33) | copy-start | bytes 24580
  315.7 8.3 %copy-start.1 = (bf16[2,192,2048]{2,1,0:T(8,128)(2,1)S(1)}, bf16[2,192,2048]{2,1,0:T(8,128)(2,1)}, u32[]{:S(2)}) copy-start(bf16[2,192,2048]{2,1,0:T(8,128)(2,1)} %param.29) | copy-start | bytes 4718596
Sparse Core Ops, SparseCore 0:
  27.9 23.9 all-gather.4
  73.4 57.2 all-gather.2
  170.6 84.3 reduce-scatter.1
